TPU v7x, 128 devices: a whole 4x4x4 slice. The times are simulated.
128 devices in a mesh: ep: 32 (over z, y, core), tp: 4 (over x).
Axes of the slice: x: 4, y: 4, z: 4, core: 2. Of those that a mesh axis runs over, the one named last changes fastest.
Arguments:
- tokens: bfloat16 [16384, 2048], P(('ep', 'tp')), may hold values from -6 to 6
- norm_gain: float32 [2048], replicated, may hold values from 0.1 to 1.9
- expert_ids: int32 [16384, 2], P('ep'), may hold values from 0 to 31, all different within a row; in each aligned block of 128 rows (0 to 127, 128 to 255, ...) at most 10 rows name the same one
- route_weight: float32 [16384, 2], P('ep'), may hold values from 0.1 to 1
- exp_gate: bfloat16 [32, 2048, 7168], P('ep', None, 'tp'), may hold values from -0.125 to 0.125
- exp_up: bfloat16 [32, 2048, 7168], P('ep', None, 'tp'), may hold values from -0.125 to 0.125
- exp_down: bfloat16 [32, 7168, 2048], P('ep', 'tp'), may hold values from -0.0625 to 0.0625
Outputs:
- mixed: bfloat16 [16384, 2048], P(('ep', 'tp'))
Inputs may be any that keep to these rules, and one draw needn't show every extreme that they name: `expert_ids`: A row names 2 different experts. Within each aligned block of 128 rows (the tokens of one device) no expert is named by more than 10 rows, and in some block one expert is named by exactly 10 rows.
All inputs are finite; a program needn't handle non-finite values.
Results may differ from a plain program's by a relative error of at most 0.012.
Values may be sent and summed in bfloat16 or wider, within the bound.
A program may use at most 128 MiB of HBM per device.

v0:
```python
import jax
import jax.numpy as jnp
from jax import lax
from jax.sharding import Mesh
from jax.sharding import PartitionSpec as P

TOPK = 2
TOK_DEV = 128
EP = ("ep_0", "ep_1", "ep_2")
EP_TP = ("ep_0", "ep_1", "ep_2", "tp")


norm_eps = 1e-05


def cut_along(value, dim, size):
    lengths = value.shape
    tiles = value.reshape(*lengths[:dim], size, lengths[dim] // size, *lengths[dim + 1 :])
    return jnp.moveaxis(tiles, dim, 0)


def in_order(tiles, dim):
    lengths = list(tiles.shape[1:])
    lengths[dim] *= tiles.shape[0]
    return jnp.moveaxis(tiles, 0, dim).reshape(lengths)


def moved_by_axis(tiles, axes, turns):
    inside = tiles.shape[1:]
    filled = tiles.reshape(*(lax.axis_size(a) for a in axes), *inside)
    for k in turns:
        filled = lax.all_to_all(filled, axes[k], k, k, tiled=True)
    return filled.reshape(-1, *inside)


def two_step_exchange(value, groups, turns, split_dim, concat_dim):
    size = lax.axis_size(groups[0]) * lax.axis_size(groups[1])
    tiles = cut_along(value, split_dim, size)
    return in_order(moved_by_axis(tiles, groups, turns), concat_dim)


def work_in_pieces(value, axis, dim, work, out_dim):
    rows = value.shape[dim]
    pieces = jnp.split(value, 2, axis=dim) if rows % 2 == 0 else [value]
    initial = jnp.arange(lax.axis_size(axis)) * rows
    tiles = [lax.all_gather(slab, axis) for slab in pieces]
    made = [jax.vmap(work)(b, initial + k * (rows // len(pieces))) for k, b in enumerate(tiles)]
    return in_order(jnp.concatenate(made, axis=out_dim + 1), out_dim)


def normalize(tokens, norm_gain):
    values = tokens.astype(jnp.float32)
    factor = lax.rsqrt(jnp.mean(values * values, axis=-1, keepdims=True) + norm_eps)
    return (values * factor * norm_gain).astype(jnp.bfloat16)


def count_slots(flat_ids, experts_all):
    onehot = (flat_ids[..., None] == jnp.arange(experts_all, dtype=jnp.int32)).astype(jnp.int32)
    before = jnp.cumsum(onehot, axis=1) - onehot
    return jnp.sum(before * onehot, axis=-1)


def expert_hidden(inputs, exp_gate, exp_up):
    gate = jnp.einsum("nerd,edf->nerf", inputs, exp_gate, preferred_element_type=jnp.float32)
    up_val = jnp.einsum("nerd,edf->nerf", inputs, exp_up, preferred_element_type=jnp.float32)
    return (jax.nn.silu(gate) * up_val).astype(jnp.bfloat16)


def per_device(tokens, norm_gain, expert_ids, route_weight, exp_gate, exp_up, exp_down):
    ep_size = lax.axis_size(EP)
    experts_all = exp_gate.shape[0] * ep_size
    capacity = (5 * TOK_DEV * TOPK + 4 * experts_all - 1) // (4 * experts_all)
    tok_count = tokens.shape[0]
    width = tokens.shape[1]
    normed = normalize(tokens, norm_gain)
    offset = lax.axis_index("tp") * tok_count
    own_ids = lax.dynamic_slice_in_dim(expert_ids, offset, tok_count, 0)
    own_weight = lax.dynamic_slice_in_dim(route_weight, offset, tok_count, 0)
    own_slots = count_slots(own_ids.reshape(1, tok_count * TOPK), experts_all).reshape(
        tok_count, TOPK
    )
    own_target = own_ids * capacity + own_slots
    copies = jnp.repeat(normed, TOPK, axis=0)
    filled = jnp.zeros((experts_all * capacity, width), jnp.bfloat16)
    filled = filled.at[own_target.reshape(-1)].set(copies)
    filled = filled.reshape(experts_all, capacity, width)
    arrived = two_step_exchange(filled, (("ep_0", "ep_1"), "ep_2"), (1, 0), 0, 1)

    def gate_piece(piece, start):
        return expert_hidden(piece, exp_gate, exp_up)

    hidden = work_in_pieces(arrived[None], "tp", 0, gate_piece, 0)
    summed = lax.psum_scatter(
        jnp.einsum("nerf,efd->nerd", hidden, exp_down, preferred_element_type=jnp.float32).astype(
            jnp.bfloat16
        ),
        "tp",
        scatter_dimension=0,
        tiled=True,
    ).astype(jnp.float32)
    expert_out = summed[0].astype(jnp.bfloat16)
    returned = two_step_exchange(expert_out, (("ep_0", "ep_1"), "ep_2"), (1, 0), 1, 0)
    flat_out = returned.reshape(experts_all * capacity, width)
    picked = flat_out[own_target].astype(jnp.float32)
    mixed = jnp.sum(own_weight[:, :, None] * picked, axis=1)
    return mixed.astype(jnp.bfloat16)


def solution(mesh):
    finer = Mesh(mesh.devices.reshape(4, 4, 2, mesh.shape["tp"]), ("ep_0", "ep_1", "ep_2", "tp"))
    return jax.shard_map(
        per_device,
        mesh=finer,
        in_specs=(
            P(EP_TP, None),
            P(),
            P(EP, None),
            P(EP, None),
            P(EP, None, "tp"),
            P(EP, None, "tp"),
            P(EP, "tp", None),
        ),
        out_specs=P(EP_TP, None),
        check_vma=False,
    )
```

profile of v0, /device:TPU:0, one launch (start us, length us, event | category | flops | bytes accessed | tf_op | source)
XLA Modules:
  0.0 259.0 jit_solution(10487113226537594660)
XLA Ops:
  6.5 0.0 copy-start
  6.5 0.0 all-gather.2.cloned.1.call-start
  6.5 0.7 copy-done
  7.2 0.1 copy.26
  7.3 0.1 eq.27
  7.5 0.6 reduce-window.6
  8.1 0.2 slice_reduce_fusion
  8.4 0.1 copy.19
  8.5 0.1 broadcast.77
  8.6 0.1 fusion.24
  8.7 0.1 reshape.204
  8.8 0.1 reshape.205
  9.0 1.2 fusion.19
  10.2 1.2 fusion.21
  11.5 0.6 broadcast_in_dim.7
  12.1 0.4 reshape.224
  12.5 2.5 scatter_custom_fusion
  15.1 0.5 reshape_reshape_reshape.6
  15.5 0.7 copy.20
  16.3 4.8 %all_to_all.20 = bf16[16,2,1,10,2048]{4,0,3,2,1:T(8,128)(2,1)S(1)} all-to-all(bf16[16,2,1,10,2048]{4,0,3,2,1:T(8,128)(2,1)S(1)} %copy.20), channel_id=1, replica_groups=mesh['ep_0'=4,'ep_1'=4,'ep_2'=2,'tp'=4] {'ep_2'}, dimensions={1} | all-to-all | bytes 2621440 | tf_op jit(solution)/shard_map/all_to_all | solution.py:32
  21.0 1.3 copy.21
  22.4 28.2 %all_to_all.21 = bf16[16,2,1,10,2048]{4,1,3,2,0:T(2,128)(2,1)S(1)} all-to-all(bf16[16,2,1,10,2048]{4,1,3,2,0:T(2,128)(2,1)S(1)} %copy.21), channel_id=1, replica_groups=mesh['ep_0'=4,'ep_1'=4,'ep_2'=2,'tp'=4] {'ep_0','ep_1'}, dimensions={0} | all-to-all | bytes 2621440 | tf_op jit(solution)/shard_map/all_to_all | solution.py:32
  50.6 0.6 copy.22
  51.3 1.3 all_gather_broadcast_in_dim_reshape_transpose_reshape.3
  52.6 0.0 all-gather.2.cloned.1.call-update
  52.6 0.2 reduce-scatter.2.cloned.1.call-start
  52.9 54.2 %all-gather.2.cloned.1.call-done = bf16[4,1,1,320,2048]{4,3,2,1,0:T(8,128)(2,1)} async-done(((bf16[1,1,1,320,2048]{4,3,2,1,0:T(8,128)(2,1)}), bf16[4,1,1,320,2048]{4,3,2,1,0:T(8,128)(2,1)}) %all-gather.2.cloned.1.call-update) | async-done | bytes 5242896 | tf_op jit(solution)/shard_map/all_gather | solution.py:46
  107.1 0.0 copy-start.2
  107.1 0.0 slice-start
  107.1 13.8 %fusion.6 = f32[4,320,1792]{2,1,0:T(8,128)S(1)} fusion(bf16[1,2048,1792]{2,1,0:T(8,128)(2,1)} %param.12, bf16[4,1,1,320,2048]{4,3,2,1,0:T(8,128)(2,1)} %all-gather.2.cloned.1.call-done), kind=kOutput, calls=%fused_computation.11 | convolution fusion | flops 9395240960 | bytes 21757952 | tf_op jit(solution)/shard_map/vmap(nerd,edf->nerf)/dot_general | solution.py:65
  121.0 0.0 copy-done.2
  121.0 0.0 slice-start.1
  121.0 15.2 %fusion = bf16[4,1,1,320,1792]{4,3,0,1,2:T(8,128)(2,1)} fusion(f32[4,320,1792]{2,1,0:T(8,128)S(1)} %fusion.6, bf16[1,2048,1792]{2,1,0:T(8,128)(2,1)} %param.11, bf16[4,1,1,320,2048]{4,3,2,1,0:T(8,128)(2,1)S(1)} %copy-done.2), kind=kOutput, calls=%fused_computation.3 | convolution fusion | flops 9409003520 | bytes 26345472 | tf_op jit(solution)/shard_map/vmap(nerd,edf->nerf)/dot_general | solution.py:64
  136.2 0.0 slice-done
  136.2 0.0 slice-done.1
  136.2 13.0 %convert_bitcast_fusion = bf16[4,1,320,2048]{3,2,0,1:T(8,128)(2,1)} fusion(bf16[1,1792,2048]{2,1,0:T(8,128)(2,1)S(1)} %bitcast.86, bf16[4,1,1,320,1792]{4,3,0,1,2:T(8,128)(2,1)} %fusion), kind=kOutput, calls=%fused_computation.17 | convolution fusion | flops 9397862400 | bytes 17170432 | tf_op jit(solution)/shard_map/nerf,efd->nerd/dot_general | solution.py:94
  149.2 0.0 reduce-scatter.2.cloned.1.call-update
  149.2 56.0 %reduce-scatter.2.cloned.1.call-done = bf16[1,1,320,2048]{3,2,0,1:T(8,128)(2,1)} async-done(((bf16[4,1,320,2048]{3,2,0,1:T(8,128)(2,1)}), bf16[1,1,320,2048]{3,2,0,1:T(8,128)(2,1)}) %reduce-scatter.2.cloned.1.call-update) | async-done | bytes 1310736 | tf_op jit(solution)/shard_map/reduce_scatter | solution.py:93
  205.3 2.3 convert_element_type.60
  207.6 0.7 copy.23
  208.3 4.8 %all_to_all.22 = bf16[16,2,1,10,2048]{4,0,3,2,1:T(8,128)(2,1)S(1)} all-to-all(bf16[16,2,1,10,2048]{4,0,3,2,1:T(8,128)(2,1)S(1)} %copy.23), channel_id=1, replica_groups=mesh['ep_0'=4,'ep_1'=4,'ep_2'=2,'tp'=4] {'ep_2'}, dimensions={1} | all-to-all | bytes 2621440 | tf_op jit(solution)/shard_map/all_to_all | solution.py:32
  213.1 2.4 copy.24
  215.5 7.0 %all-to-all-start.3 = ((bf16[16,2,1,10,2048]{4,1,3,2,0:T(2,128)(2,1)}), bf16[16,2,1,10,2048]{4,1,3,2,0:T(2,128)(2,1)S(1)}, u32[]{:S(2)}, u32[]{:S(2)}) async-start(bf16[16,2,1,10,2048]{4,1,3,2,0:T(2,128)(2,1)} %copy.24), calls=%async_computation.4 | async-start | bytes 2621440 | tf_op jit(solution)/shard_map/all_to_all | solution.py:32
  222.5 0.1 reshape.214
  222.6 0.7 constant_dynamic-slice_fusion.1
  223.3 0.1 copy.15
  223.4 20.8 %all-to-all-done.3 = bf16[16,2,1,10,2048]{4,1,3,2,0:T(2,128)(2,1)S(1)} async-done(((bf16[16,2,1,10,2048]{4,1,3,2,0:T(2,128)(2,1)}), bf16[16,2,1,10,2048]{4,1,3,2,0:T(2,128)(2,1)S(1)}, u32[]{:S(2)}, u32[]{:S(2)}) %all-to-all-start.3) | async-done | bytes 1310752 | tf_op jit(solution)/shard_map/all_to_all | solution.py:32
  244.3 0.6 copy.25
  244.9 0.5 reshape_reshape_reshape.7
  245.4 0.0 copy-start.1
  245.4 1.4 gather_fusion
  246.8 1.3 reshape.230
  248.2 4.0 %multiply_reduce_fusion = bf16[128,2048]{1,0:T(8,128)(2,1)} fusion(f32[128,2,2048]{2,1,0:T(2,128)S(1)} %reshape.230, f32[128,2]{1,0:T(8,128)S(1)} %copy.15), kind=kLoop, calls=%fused_computation.19 | loop fusion | flops 786432 | bytes 2622464 | tf_op jit(solution)/shard_map/reduce_sum | solution.py:105
  252.2 0.0 copy-done.1
  (11 shorter events, 0.1 us)
Async XLA Ops:
  6.5 0.7 copy-start
  6.5 100.6 %all-gather.2.cloned.1.call-start = ((), (), s32[]{:S(2)}) async-start(), calls=%async_computation.5 | async-start | bytes 6553600 | tf_op jit(solution)/shard_map/all_gather | solution.py:46
  52.6 152.6 %reduce-scatter.2.cloned.1.call-start = ((), (), s32[]{:S(2)}) async-start(), calls=%async_computation.6 | async-start | bytes 6553600 | tf_op jit(solution)/shard_map/reduce_scatter | solution.py:93
  107.1 13.9 %copy-start.2 = (bf16[4,1,1,320,2048]{4,3,2,1,0:T(8,128)(2,1)S(1)}, bf16[4,1,1,320,2048]{4,3,2,1,0:T(8,128)(2,1)}, u32[]{:S(2)}) copy-start(bf16[4,1,1,320,2048]{4,3,2,1,0:T(8,128)(2,1)} %all-gather.2.cloned.1.call-done) | copy-start | bytes 15728644
  107.1 29.1 %slice-start = ((s8[7340032]{0:T(1024)(128)(4,1)}), s8[4194304]{0:T(1024)(128)(4,1)S(1)}, s32[]{:S(2)}) async-start(s8[7340032]{0:T(1024)(128)(4,1)} %bitcast.85), calls=%async_computation.7 | async-start | bytes 8388608
  121.0 15.3 %slice-start.1 = ((s8[7340032]{0:T(1024)(128)(4,1)}), s8[3145728]{0:T(1024)(128)(4,1)S(1)}, s32[]{:S(2)}) async-start(s8[7340032]{0:T(1024)(128)(4,1)} %bitcast.85), calls=%async_computation.8 | async-start | bytes 6291456
  215.5 28.8 %all-to-all-start.3 = ((bf16[16,2,1,10,2048]{4,1,3,2,0:T(2,128)(2,1)}), bf16[16,2,1,10,2048]{4,1,3,2,0:T(2,128)(2,1)S(1)}, u32[]{:S(2)}, u32[]{:S(2)}) async-start(bf16[16,2,1,10,2048]{4,1,3,2,0:T(2,128)(2,1)} %copy.24), calls=%async_computation.4 | async-start | bytes 2621440 | tf_op jit(solution)/shard_map/all_to_all | solution.py:32
  245.4 6.8 %copy-start.1 = (s32[512,2]{0,1:T(2,128)S(1)}, s32[512,2]{0,1:T(2,128)}, u32[]{:S(2)}) copy-start(s32[512,2]{0,1:T(2,128)} %param.9) | copy-start | bytes 12292
Sparse Core Ops, SparseCore 0:
  52.8 54.3 all-gather.1
  149.4 55.8 reduce-scatter.1
where the time goes:
time: 259 us
  waiting for transfers between devices  131 us (51%)
  matrix products  42.1 us (16%)
  blocking collectives  37.8 us (15%)
  local copies, waits for them, and re-layouts  19.9 us (8%)
  between operations  13.6 us (5%)
  other arithmetic  7.28 us (3%)
  starting transfers between devices  7.2 us (3%)
    reduce_scatter x1, waiting for transfers between devices, per_device(): lax.psum_scatter(jnp.einsum('nerf,efd->nerd', hidden, exp_down, preferred...  56 us
    all_gather x1, waiting for transfers between devices, work_in_pieces(): tiles = [lax.all_gather(slab, axis) for slab in pieces]  54.2 us
    all_to_all x3, blocking collectives, moved_by_axis(): filled = lax.all_to_all(filled, axes[k], k, k, tiled=True)  37.8 us
    all_to_all x1, waiting for transfers between devices, moved_by_axis(): filled = lax.all_to_all(filled, axes[k], k, k, tiled=True)  20.8 us
    dot_general x1, matrix products, expert_hidden(): jnp.einsum('nerd,edf->nerf', inputs, exp_gate, preferred_element_type=jnp...  15.2 us
    dot_general x1, matrix products, expert_hidden(): jnp.einsum('nerd,edf->nerf', inputs, exp_up, preferred_element_type=jnp.f...  13.8 us
    dot_general x1, matrix products, per_device(): jnp.einsum('nerf,efd->nerd', hidden, exp_down, preferred_element_type=jnp...  13 us
    all_to_all x1, starting transfers between devices, moved_by_axis(): filled = lax.all_to_all(filled, axes[k], k, k, tiled=True)  6.97 us
  transfers between devices with their start and end apart: 3, of which 3 were waited for; matrix products, arithmetic and copies ran while one was open for 0% of the time, Pallas kernels for 0%

commit v1 on v0

v1 whole, which is shorter than its diff:
```python
import jax
import jax.numpy as jnp
from jax import lax
from jax.experimental import pallas as pl
from jax.experimental.pallas import tpu as pltpu
from jax.sharding import PartitionSpec as P

TOP = 2
CAP = 10
EPS = 1e-05
Z, YC, TP = 4, 8, 4
PAIRS = CAP // 2
OFFSETS = (0, 1, 3, 2)
MESH = pl.DeviceIdType.MESH
BF16, F32 = jnp.bfloat16, jnp.float32


def kernel(
    ids_ref, weight_ref, tok_ref, gain_ref, gate_hbm, up_hbm, down_hbm, out_ref,
    w_gate, w_up, w_down, own_n, side_n, fill_o, fill_s, got, part, rows, hidden,
    ret_o, ret_s, back_o, back_s, rows_s, mix_out, mix_in,
    w_sem, pre_s, pre_r, yz_s, yz_r, xp_s, xp_r, xr_s, xr_r, yb_s, yb_r, fin_s, fin_r,
):
    me, x = lax.axis_index("ep"), lax.axis_index("tp")
    z, yc = me // YC, me % YC
    xr, xl, xo = (x + 1) % TP, (x + 3) % TP, (x + 2) % TP
    half = own_n.shape[2]
    toks = own_n.shape[1]
    side = (xl, xr)
    cols = (pl.ds(0, half), pl.ds(half, half))
    group = YC * CAP

    loads = [
        pltpu.make_async_copy(src.at[0], dst, w_sem.at[i])
        for i, (src, dst) in enumerate(((gate_hbm, w_gate), (up_hbm, w_up), (down_hbm, w_down)))
    ]
    for load in loads:
        load.start()

    barrier = pltpu.get_barrier_semaphore()

    @pl.loop(1, Z * YC)
    def _(i):
        pl.semaphore_signal(barrier, inc=1, device_id=((me + i) % (Z * YC), x), device_id_type=MESH)

    for peer in (xl, xr):
        pl.semaphore_signal(barrier, inc=1, device_id=(me, peer), device_id_type=MESH)

    def remote(src, dst, send, recv, ep, tp):
        return pltpu.make_async_remote_copy(
            src_ref=src, dst_ref=dst, send_sem=send, recv_sem=recv, device_id=(ep, tp), device_id_type=MESH
        )

    @pl.loop(0, toks // 32)
    def _(i):
        at = pl.ds(pl.multiple_of(i * 32, 32), 32)
        v = tok_ref[at, :].astype(F32)
        factor = lax.rsqrt(jnp.mean(v * v, axis=-1, keepdims=True) + EPS)
        n = (v * factor * gain_ref[...]).astype(BF16)
        own_n[0, at, :] = n[:, :half]
        own_n[1, at, :] = n[:, half:]

    pl.semaphore_wait(barrier, Z * YC - 1 + 2)
    pres = [
        remote(own_n.at[0], side_n.at[0], pre_s.at[0], pre_r.at[0], me, xr),
        remote(own_n.at[1], side_n.at[1], pre_s.at[1], pre_r.at[1], me, xl),
    ]
    for copy in pres:
        copy.start()

    def targets(at):
        pair = ids_ref[at]
        e = lax.broadcasted_iota(jnp.int32, (Z * YC, toks), 0)
        before = lax.broadcasted_iota(jnp.int32, (toks, toks), 0) < lax.broadcasted_iota(jnp.int32, (toks, toks), 1)
        named = [e == pair[k : k + 1, :] for k in range(TOP)]
        member = (named[0] | named[1]).astype(F32).astype(BF16)
        count = jnp.dot(member, before.astype(F32).astype(BF16), preferred_element_type=F32)
        slots = [jnp.sum(jnp.where(n, count, 0.0), axis=0, keepdims=True).astype(jnp.int32) for n in named]
        return [pair[k : k + 1, :] * CAP + slots[k] for k in range(TOP)]

    def pick(where, base):
        r = lax.broadcasted_iota(jnp.int32, (group, toks), 0) + base
        return ((r == where[0]) | (r == where[1])).astype(F32).astype(BF16)

    def filled(onehot, values):
        return jnp.dot(onehot, values, preferred_element_type=F32).astype(BF16).reshape(YC, PAIRS, 2, half)

    where_own = targets(x)
    for q in range(Z):
        ze = (z + Z - OFFSETS[q]) % Z
        onehot = pick(where_own, ze * group)
        for h in range(2):
            fill_o[ze, :, :, :, cols[h]] = filled(onehot, own_n[h])
        if q == 0:
            got[x, z, yc] = fill_o[z, yc]

        @pl.loop(1 if q == 0 else 0, YC)
        def _(i):
            j = (yc + i) % YC
            remote(fill_o.at[ze, j], got.at[x, z, yc], yz_s.at[0, q], yz_r.at[0, q], ze * YC + j, x).start()

    where_side = [targets(side[h]) for h in range(2)]
    for copy in pres:
        copy.wait()
    for q in range(Z):
        ze = (z + Z - OFFSETS[q]) % Z
        for h in range(2):
            fill_s[h, ze] = filled(pick(where_side[h], ze * group), side_n[h])
            if q == 0:
                got[side[h], z, yc, :, :, cols[h]] = fill_s[h, z, yc]

        @pl.loop(1 if q == 0 else 0, YC)
        def _(i):
            j = (yc + i) % YC
            for h in range(2):
                remote(
                    fill_s.at[h, ze, j], got.at[side[h], z, yc, :, :, cols[h]],
                    yz_s.at[1 + h, q], yz_r.at[1 + h, q], ze * YC + j, x,
                ).start()

    def source(q):
        return (z + OFFSETS[q]) % Z

    def posts(q):
        zs = source(q)
        plan = ((x, 0, xl), (x, 1, xr), (xl, 0, xr), (xr, 1, xl))
        return [
            remote(
                got.at[t, zs, :, :, :, cols[h]], got.at[t, zs, :, :, :, cols[h]],
                xp_s.at[k, q], xp_r.at[k, q], me, to,
            )
            for k, (t, h, to) in enumerate(plan)
        ]

    def drained(view, send, recv, q):
        count = YC - 1 if q == 0 else YC
        return remote(view.at[pl.ds(0, count)], view.at[pl.ds(0, count)], send, recv, me, xr)

    def forward(q):
        drained(fill_o.at[0], yz_s.at[0, q], yz_r.at[0, q], q).wait_recv()
        copies = posts(q)
        copies[0].start()
        copies[1].start()
        for h in range(2):
            drained(fill_s.at[h, 0], yz_s.at[1 + h, q], yz_r.at[1 + h, q], q).wait_recv()
            copies[2 + h].start()

    def returns(q):
        zs = source(q)
        return [
            remote(part.at[xr, zs, :, :, :, cols[0]], ret_o.at[zs, :, :, :, cols[0]], xr_s.at[0, q], xr_r.at[0, q], me, xr),
            remote(part.at[xo, zs, :, :, :, cols[0]], ret_s.at[0, zs], xr_s.at[1, q], xr_r.at[1, q], me, xl),
            remote(part.at[xl, zs, :, :, :, cols[1]], ret_o.at[zs, :, :, :, cols[1]], xr_s.at[2, q], xr_r.at[2, q], me, xl),
            remote(part.at[xo, zs, :, :, :, cols[1]], ret_s.at[1, zs], xr_s.at[3, q], xr_r.at[3, q], me, xr),
        ]

    def up_phase(q):
        zs = source(q)
        for t in range(TP):
            rows[pl.ds(t * group, group), :] = got[t, zs].reshape(group, 2 * half)
        if q == 0:
            loads[0].wait()
            loads[1].wait()

        @pl.loop(0, hidden.shape[1] // 256)
        def _(n):
            at = pl.ds(pl.multiple_of(n * 256, 256), 256)
            gate = jnp.dot(rows[...], w_gate[:, at], preferred_element_type=F32)
            up = jnp.dot(rows[...], w_up[:, at], preferred_element_type=F32)
            hidden[:, at] = (gate / (1.0 + jnp.exp(-gate)) * up).astype(BF16)

        if q == 0:
            loads[2].wait()

    def down_phase(q, h):
        zs = source(q)
        tiles = half // 256

        @pl.loop(h * tiles, (h + 1) * tiles)
        def _(n):
            at = pl.ds(pl.multiple_of(n * 256, 256), 256)
            o = jnp.dot(hidden[...], w_down[:, at], preferred_element_type=F32).astype(BF16)
            for t in range(TP):
                part[t, zs, :, :, :, at] = o[t * group : (t + 1) * group].reshape(YC, PAIRS, 2, 256)

    def give_back(q):
        zs = source(q)
        for copy in returns(q):
            copy.wait_recv()

        def summed(a, b):
            return (a.astype(F32) + b.astype(F32)).astype(BF16)

        @pl.loop(0, YC)
        def _(j):
            part[x, zs, j] = summed(part[x, zs, j], ret_o[zs, j])
            for h in range(2):
                part[side[h], zs, j, :, :, cols[h]] = summed(part[side[h], zs, j, :, :, cols[h]], ret_s[h, zs, j])

        if q == 0:
            back_o[z, yc] = part[x, z, yc]
            for h in range(2):
                back_s[h, z, yc] = part[side[h], z, yc, :, :, cols[h]]

        @pl.loop(1 if q == 0 else 0, YC)
        def _(i):
            j = (yc + i) % YC
            remote(part.at[x, zs, j], back_o.at[z, yc], yb_s.at[0, q], yb_r.at[0, q], zs * YC + j, x).start()
            for h in range(2):
                remote(
                    part.at[side[h], zs, j, :, :, cols[h]], back_s.at[h, z, yc],
                    yb_s.at[1 + h, q], yb_r.at[1 + h, q], zs * YC + j, x,
                ).start()

    forward(0)
    forward(1)
    for q in range(Z):
        for copy in posts(q):
            copy.wait_recv()
        up_phase(q)
        if q + 2 < Z:
            forward(q + 2)
        if q >= 1:
            give_back(q - 1)
        down_phase(q, 0)
        copies = returns(q)
        copies[0].start()
        copies[1].start()
        down_phase(q, 1)
        copies[2].start()
        copies[3].start()
    give_back(Z - 1)

    def spread(at, where):
        r = lax.broadcasted_iota(jnp.int32, (Z * group, toks), 0)
        w = weight_ref[at]
        full = jnp.where(r == where[0], w[0:1, :], 0.0) + jnp.where(r == where[1], w[1:2, :], 0.0)
        high = full.astype(BF16)
        return high, (full - high.astype(F32)).astype(BF16)

    def mixed(spreads, values):
        dims = (((0,), (0,)), ((), ()))
        return sum(lax.dot_general(s, values, dims, preferred_element_type=F32) for s in spreads)

    spreads = [spread(side[h], where_side[h]) for h in range(2)]
    finals = [
        remote(mix_out.at[0], mix_in.at[0], fin_s.at[0], fin_r.at[0], me, xl),
        remote(mix_out.at[1], mix_in.at[1], fin_s.at[1], fin_r.at[1], me, xr),
    ]
    for h in range(2):
        for q in range(Z):
            drained(fill_s.at[h, 0], yb_s.at[1 + h, q], yb_r.at[1 + h, q], q).wait_recv()
        for zz in range(Z):
            rows_s[h, pl.ds(zz * group, group), :] = back_s[h, zz].reshape(group, half)
        mix_out[h] = mixed(spreads[h], rows_s[h]).astype(BF16)
        finals[h].start()
    for q in range(Z):
        drained(fill_o.at[0], yb_s.at[0, q], yb_r.at[0, q], q).wait_recv()
    for zz in range(Z):
        rows[pl.ds(zz * group, group), :] = back_o[zz].reshape(group, 2 * half)
    spread_own = spread(x, where_own)
    for h in range(2):
        value = mixed(spread_own, rows[:, cols[h]])
        finals[h].wait()
        out_ref[:, cols[h]] = (value + mix_in[h].astype(F32)).astype(BF16)

    for q in range(Z):
        for copy in posts(q) + returns(q):
            copy.wait_send()
        for send in (yz_s, yb_s):
            for k, view in enumerate((fill_o.at[0], fill_s.at[0, 0], fill_s.at[1, 0])):
                drained(view, send.at[k, q], send.at[k, q], q).wait_send()


def per_device(tokens, norm_gain, expert_ids, route_weight, exp_gate, exp_up, exp_down):
    toks, width = tokens.shape
    half = width // 2
    inner = exp_gate.shape[2]
    ids = expert_ids.reshape(TP, toks, TOP).transpose(0, 2, 1)
    weight = route_weight.reshape(TP, toks, TOP).transpose(0, 2, 1)
    vmem, hbm = pl.BlockSpec(memory_space=pltpu.VMEM), pl.BlockSpec(memory_space=pl.ANY)
    dma = pltpu.SemaphoreType.DMA
    full, part = (YC, PAIRS, 2, width), (YC, PAIRS, 2, half)
    group = YC * CAP
    return pl.pallas_call(
        kernel,
        out_shape=jax.ShapeDtypeStruct((toks, width), BF16),
        in_specs=[vmem] * 4 + [hbm] * 3,
        out_specs=vmem,
        scratch_shapes=[
            pltpu.VMEM((width, inner), BF16),
            pltpu.VMEM((width, inner), BF16),
            pltpu.VMEM((inner, width), BF16),
            pltpu.VMEM((2, toks, half), BF16),
            pltpu.VMEM((2, toks, half), BF16),
            pltpu.VMEM((Z,) + full, BF16),
            pltpu.VMEM((2, Z) + part, BF16),
            pltpu.VMEM((TP, Z) + full, BF16),
            pltpu.VMEM((TP, Z) + full, BF16),
            pltpu.VMEM((TP * group, width), BF16),
            pltpu.VMEM((TP * group, inner), BF16),
            pltpu.VMEM((Z,) + full, BF16),
            pltpu.VMEM((2, Z) + part, BF16),
            pltpu.VMEM((Z,) + full, BF16),
            pltpu.VMEM((2, Z) + part, BF16),
            pltpu.VMEM((2, Z * group, half), BF16),
            pltpu.VMEM((2, toks, half), BF16),
            pltpu.VMEM((2, toks, half), BF16),
            dma((3,)),
            dma((2,)),
            dma((2,)),
            dma((3, Z)),
            dma((3, Z)),
            dma((4, Z)),
            dma((4, Z)),
            dma((4, Z)),
            dma((4, Z)),
            dma((3, Z)),
            dma((3, Z)),
            dma((2,)),
            dma((2,)),
        ],
        compiler_params=pltpu.CompilerParams(
            collective_id=0, has_side_effects=True, vmem_limit_bytes=63 * 2**20
        ),
    )(ids, weight, tokens, norm_gain.reshape(1, width), exp_gate, exp_up, exp_down)


def solution(mesh):
    return jax.shard_map(
        per_device,
        mesh=mesh,
        in_specs=(
            P(("ep", "tp"), None),
            P(),
            P("ep", None),
            P("ep", None),
            P("ep", None, "tp"),
            P("ep", None, "tp"),
            P("ep", "tp", None),
        ),
        out_specs=P(("ep", "tp"), None),
        check_vma=False,
    )
```

time: 259 us -> 129 us (0.50)
  waiting for transfers between devices: 131 us -> 0 us
  Pallas kernels: 0 us -> 126 us
  matrix products: 42.1 us -> 0 us
  blocking collectives: 37.8 us -> 0 us
  local copies, waits for them, and re-layouts: 19.9 us -> 1.88 us
  between operations: 13.6 us -> 0.01 us
  other arithmetic: 7.28 us -> 0 us
  starting transfers between devices: 7.2 us -> 0 us
    pallas_call x0 -> x1, Pallas kernels: none -> 126 us  [per_device(): pl.pallas_call(kernel, out_shape=jax.ShapeDtypeStruct((toks, width), BF16...]
    reduce_scatter x1 -> x0, waiting for transfers between devices: 56 us -> none  [per_device(): lax.psum_scatter(jnp.einsum('nerf,efd->nerd', hidden, exp_down, preferred...]
    all_gather x1 -> x0, waiting for transfers between devices: 54.2 us -> none  [work_in_pieces(): tiles = [lax.all_gather(slab, axis) for slab in pieces]]
    dot_general x3 -> x0, matrix products: 42.1 us -> none  [the longest x1 15.2 us: expert_hidden(): jnp.einsum('nerd,edf->nerf', inputs, exp_gate, preferred_element_type=jnp...]
    all_to_all x3 -> x0, blocking collectives: 37.8 us -> none  [moved_by_axis(): filled = lax.all_to_all(filled, axes[k], k, k, tiled=True)]
    all_to_all x1 -> x0, waiting for transfers between devices: 20.8 us -> none  [moved_by_axis(): filled = lax.all_to_all(filled, axes[k], k, k, tiled=True)]
    all_to_all x1 -> x0, starting transfers between devices: 6.97 us -> none  [moved_by_axis(): filled = lax.all_to_all(filled, axes[k], k, k, tiled=True)]
    reduce_sum x3 -> x0, other arithmetic: 5.35 us -> none  [the longest x1 4.04 us: per_device(): mixed = jnp.sum(own_weight[:, :, None] * picked, axis=1)]
  transfers between devices with their start and end apart: 3 -> 0, of which waited for: 3 -> 0; matrix products, arithmetic and copies ran while one was open for 0% -> 0% of each run, Pallas kernels for 0% -> 0%
where the time goes in v1:
time: 129 us; the launch traced here: 128 us
  Pallas kernels  126 us (98%)
  local copies, waits for them, and re-layouts  1.88 us (1%)
    pallas_call x1, Pallas kernels, per_device(): pl.pallas_call(kernel, out_shape=jax.ShapeDtypeStruct((toks, width), BF16...  126 us

profile of v1, /device:TPU:0, one launch (start us, length us, event | category | flops | bytes accessed | tf_op | source)
XLA Modules:
  0.0 127.5 jit_solution(17727539743567861454)
XLA Ops:
  0.0 125.6 %shard_map.73 = bf16[128,2048]{1,0:T(8,128)(2,1)} custom-call(s32[4,2,128]{2,1,0:T(2,128)} %bitcast.8, f32[4,2,128]{2,1,0:T(2,128)} %bitcast.9, bf16[128,2048]{1,0:T(8,128)(2,1)} %tok_ref.1, f32[1,2048]{1,0:T(1,128)} %bitcast.7, bf16[1,2048,1792]{2,1,0:T(8,128)(2,1)} %gate_hbm.1, bf16[1,2048,1792]{2,1,0:T(8,128)(2,1)} %up_hbm.1, bf16[1,1792,2048]{2,1,0:T(8,128)(2,1)} %down_hbm.1), custom_call_target="tpu_custom_call" | custom-call | tf_op jit(solution)/shard_map/pallas_call | solution.py:285
  125.6 1.9 %copy.9 = bf16[128,2048]{1,0:T(8,128)(2,1)} copy(bf16[128,2048]{1,0:T(8,128)(2,1)} %shard_map.73) | data formatting | bytes 1048576

commit v2 on v1

v2 whole, which is shorter than its diff:
```python
import jax
import jax.numpy as jnp
from jax import lax
from jax.experimental import pallas as pl
from jax.experimental.pallas import tpu as pltpu
from jax.sharding import PartitionSpec as P

TOP = 2
CAP = 10
EPS = 1e-05
Z, YC, TP = 4, 8, 4
PAIRS = CAP // 2
ORDER = (1, 0, 3, 2)
MESH = pl.DeviceIdType.MESH
BF16, F32 = jnp.bfloat16, jnp.float32


def kernel(
    ids_ref, weight_ref, tok_ref, gain_ref, gate_hbm, up_hbm, down_hbm, out_ref,
    w_gate, w_up, w_down, own_n, side_n, fill_o, fill_s, got, part, rows, hidden,
    ret_o, ret_s, back_o, back_s, rows_s, mix_out, mix_in,
    w_sem, pre_s, pre_r, yz_s, yz_r, xp_s, xp_r, xr_s, xr_r, yb_s, yb_r, fin_s, fin_r,
):
    me, x = lax.axis_index("ep"), lax.axis_index("tp")
    z, y, core = me // 8, me // 2 % 4, me % 2
    xr, xl, xo = (x + 1) % TP, (x + 3) % TP, (x + 2) % TP
    half = own_n.shape[2]
    toks = own_n.shape[1]
    side = (xl, xr)
    cols = (pl.ds(0, half), pl.ds(half, half))
    group = YC * CAP

    loads = [
        pltpu.make_async_copy(src.at[0], dst, w_sem.at[i])
        for i, (src, dst) in enumerate(((gate_hbm, w_gate), (up_hbm, w_up), (down_hbm, w_down)))
    ]
    for load in loads:
        load.start()

    barrier = pltpu.get_barrier_semaphore()

    @pl.loop(1, Z * YC)
    def _(i):
        pl.semaphore_signal(barrier, inc=1, device_id=((me + i) % (Z * YC), x), device_id_type=MESH)

    for peer in (xl, xr):
        pl.semaphore_signal(barrier, inc=1, device_id=(me, peer), device_id_type=MESH)

    def remote(src, dst, send, recv, ep, tp):
        return pltpu.make_async_remote_copy(
            src_ref=src, dst_ref=dst, send_sem=send, recv_sem=recv, device_id=(ep, tp), device_id_type=MESH
        )

    @pl.loop(0, toks // 32)
    def _(i):
        at = pl.ds(pl.multiple_of(i * 32, 32), 32)
        v = tok_ref[at, :].astype(F32)
        factor = lax.rsqrt(jnp.mean(v * v, axis=-1, keepdims=True) + EPS)
        n = (v * factor * gain_ref[...]).astype(BF16)
        own_n[0, at, :] = n[:, :half]
        own_n[1, at, :] = n[:, half:]

    with jax.named_scope("bar"):
        pl.semaphore_wait(barrier, Z * YC - 1 + 2)
    pres = [
        remote(own_n.at[0], side_n.at[0], pre_s.at[0], pre_r.at[0], me, xr),
        remote(own_n.at[1], side_n.at[1], pre_s.at[1], pre_r.at[1], me, xl),
    ]
    for copy in pres:
        copy.start()

    def targets(at):
        pair = ids_ref[at]
        e = lax.broadcasted_iota(jnp.int32, (Z * YC, toks), 0)
        before = lax.broadcasted_iota(jnp.int32, (toks, toks), 0) < lax.broadcasted_iota(jnp.int32, (toks, toks), 1)
        named = [e == pair[k : k + 1, :] for k in range(TOP)]
        member = (named[0] | named[1]).astype(F32).astype(BF16)
        count = jnp.dot(member, before.astype(F32).astype(BF16), preferred_element_type=F32)
        slots = [jnp.sum(jnp.where(n, count, 0.0), axis=0, keepdims=True).astype(jnp.int32) for n in named]
        dz = (z - (pair >> 3)) & 3
        k = (y - (pair >> 1) - dz) & 3
        base = ((k * 4 + dz) * 2 + (pair & 1)) * CAP
        return [base[k : k + 1, :] + slots[k] for k in range(TOP)]

    def pick(where, base):
        r = lax.broadcasted_iota(jnp.int32, (group, toks), 0) + base
        return ((r == where[0]) | (r == where[1])).astype(F32).astype(BF16)

    def filled(onehot, values):
        return jnp.dot(onehot, values, preferred_element_type=F32).astype(BF16).reshape(YC, PAIRS, 2, half)

    def each(k, sign, send):
        @pl.loop(1 if k == 0 else 0, YC)
        def _(i):
            dz, c = i // 2, (core + i) % 2
            ep = (z + 4 + sign * dz) % 4 * 8 + (y + 8 + sign * (dz + k)) % 4 * 2 + c
            send(dz * 2 + c, dz * 2 + core, ep)

    def drained(view, send, recv, k):
        count = YC - 1 if k == 0 else YC
        return remote(view.at[pl.ds(0, count)], view.at[pl.ds(0, count)], send, recv, me, xr)

    where_own = targets(x)
    for k in ORDER:
        onehot = pick(where_own, k * group)
        for h in range(2):
            fill_o[k, :, :, :, cols[h]] = filled(onehot, own_n[h])
        if k == 0:
            got[x, k, core] = fill_o[k, core]

        def send_own(j, mine, ep):
            remote(fill_o.at[k, j], got.at[x, k, mine], yz_s.at[0, k], yz_r.at[0, k], ep, x).start()

        each(k, -1, send_own)

    def posts(k):
        plan = ((x, 0, xl), (x, 1, xr), (xl, 0, xr), (xr, 1, xl))
        return [
            remote(
                got.at[t, k, :, :, :, cols[h]], got.at[t, k, :, :, :, cols[h]],
                xp_s.at[i, k], xp_r.at[i, k], me, to,
            )
            for i, (t, h, to) in enumerate(plan)
        ]

    def forward_own(k):
        with jax.named_scope("fo"):
            drained(fill_o.at[0], yz_s.at[0, k], yz_r.at[0, k], k).wait_recv()
        for copy in posts(k)[:2]:
            copy.start()

    def forward_side(k):
        for h in range(2):
            with jax.named_scope("fs"):
                drained(fill_s.at[h, 0], yz_s.at[1 + h, k], yz_r.at[1 + h, k], k).wait_recv()
            posts(k)[2 + h].start()

    where_side = [targets(side[h]) for h in range(2)]
    forward_own(ORDER[0])
    with jax.named_scope("pre"):
        for copy in pres:
            copy.wait()
    for k in ORDER:
        for h in range(2):
            fill_s[h, k] = filled(pick(where_side[h], k * group), side_n[h])
            if k == 0:
                got[side[h], k, core, :, :, cols[h]] = fill_s[h, k, core]

        def send_side(j, mine, ep):
            for h in range(2):
                remote(
                    fill_s.at[h, k, j], got.at[side[h], k, mine, :, :, cols[h]],
                    yz_s.at[1 + h, k], yz_r.at[1 + h, k], ep, x,
                ).start()

        each(k, -1, send_side)
    for k in ORDER[1:]:
        forward_own(k)

    def splits(k):
        return 2 if k == ORDER[-1] else 1

    def cut(k, h, r):
        width = half // splits(k)
        return pl.ds(h * half + r * width, width)

    def inner(k, r):
        width = half // splits(k)
        return pl.ds(r * width, width)

    def slot(k, r):
        return ORDER.index(k) + r

    def returns(k, r):
        i = slot(k, r)
        plan = ((xr, 0, 0, xr), (xo, 0, 1, xl), (xl, 1, 0, xl), (xo, 1, 1, xr))
        out = []
        for n, (t, h, kind, to) in enumerate(plan):
            dst = ret_s.at[h, k, :, :, :, inner(k, r)] if kind else ret_o.at[k, :, :, :, cut(k, h, r)]
            out.append(remote(part.at[t, k, :, :, :, cut(k, h, r)], dst, xr_s.at[n, i], xr_r.at[n, i], me, to))
        return out

    def up_phase(blocks, first):
        size = len(blocks) * group
        for i, (t, k) in enumerate(blocks):
            rows[pl.ds(i * group, group), :] = got[t, k].reshape(group, 2 * half)
        if first:
            loads[0].wait()
            loads[1].wait()
        for n in range(hidden.shape[1] // 256):
            at = pl.ds(n * 256, 256)
            gate = jnp.dot(rows[:size, :], w_gate[:, at], preferred_element_type=F32)
            up = jnp.dot(rows[:size, :], w_up[:, at], preferred_element_type=F32)
            hidden[:size, at] = (gate / (1.0 + jnp.exp(-gate)) * up).astype(BF16)
        if first:
            loads[2].wait()

    def down_phase(blocks, at):
        size = len(blocks) * group
        o = jnp.dot(hidden[:size, :], w_down[:, at], preferred_element_type=F32).astype(BF16)
        for i, (t, k) in enumerate(blocks):
            part[t, k, :, :, :, at] = o[i * group : (i + 1) * group].reshape(YC, PAIRS, 2, at.size)

    def give_back(k, r):
        with jax.named_scope("gw"):
            for copy in returns(k, r):
                copy.wait_recv()
        with jax.named_scope("gs"):

            @pl.loop(0, YC)
            def _(j):
                for h in range(2):
                    at = cut(k, h, r)
                    part[x, k, j, :, :, at] = part[x, k, j, :, :, at] + ret_o[k, j, :, :, at]
                    part[side[h], k, j, :, :, at] = part[side[h], k, j, :, :, at] + ret_s[h, k, j, :, :, inner(k, r)]

        if k == 0:
            for h in range(2):
                at = cut(k, h, r)
                back_o[k, core, :, :, at] = part[x, k, core, :, :, at]
                back_s[h, k, core, :, :, inner(k, r)] = part[side[h], k, core, :, :, at]
        i = slot(k, r)

        def send_back(j, mine, ep):
            for h in range(2):
                remote(
                    part.at[side[h], k, j, :, :, cut(k, h, r)], back_s.at[h, k, mine, :, :, inner(k, r)],
                    yb_s.at[1 + h, i], yb_r.at[1 + h, i], ep, x,
                ).start()
            for h in range(2):
                at = cut(k, h, r)
                remote(
                    part.at[x, k, j, :, :, at], back_o.at[k, mine, :, :, at],
                    yb_s.at[0, i], yb_r.at[0, i], ep, x,
                ).start()

        each(k, 1, send_back)

    own = [(x, k) for k in ORDER]
    with jax.named_scope("up0"):
        up_phase(own, True)
    forward_side(ORDER[0])
    with jax.named_scope("down0"):
        for h in range(2):
            down_phase(own, pl.ds(h * half, half))
    forward_side(ORDER[1])
    for p, k in enumerate(ORDER):
        blocks = [(t, k) for t in (xl, xr, xo)]
        with jax.named_scope("pw"):
            for copy in posts(k):
                copy.wait_recv()
        with jax.named_scope("up"):
            up_phase(blocks, False)
        if p == 0:
            forward_side(ORDER[2])
        if p >= 2:
            give_back(ORDER[p - 2], 0)
        for r in range(splits(k)):
            with jax.named_scope("dn"):
                copies = returns(k, r)
                for h in range(2):
                    down_phase(blocks, cut(k, h, r))
                    copies[2 * h].start()
                    copies[2 * h + 1].start()
        if p == 0:
            forward_side(ORDER[3])
    give_back(ORDER[2], 0)
    give_back(ORDER[3], 0)
    give_back(ORDER[3], 1)

    def spread(at, where):
        r = lax.broadcasted_iota(jnp.int32, (Z * group, toks), 0)
        w = weight_ref[at]
        full = jnp.where(r == where[0], w[0:1, :], 0.0) + jnp.where(r == where[1], w[1:2, :], 0.0)
        high = full.astype(BF16)
        return high, (full - high.astype(F32)).astype(BF16)

    def mixed(spreads, values):
        dims = (((0,), (0,)), ((), ()))
        return sum(lax.dot_general(s, values, dims, preferred_element_type=F32) for s in spreads)

    last = ORDER[-1]
    spreads = [spread(side[h], where_side[h]) for h in range(2)]
    spread_own = spread(x, where_own)

    def back_side(h, k, r):
        view = fill_s.at[h, 0, :, :, :, inner(k, r)]
        return drained(view, yb_s.at[1 + h, slot(k, r)], yb_r.at[1 + h, slot(k, r)], k)

    def back_own(k, r):
        view = fill_s.at[0, 0] if splits(k) == 2 else fill_o.at[0]
        return drained(view, yb_s.at[0, slot(k, r)], yb_r.at[0, slot(k, r)], k)

    finals = {}
    for r in range(splits(last)):
        for h in range(2):
            with jax.named_scope("bs"):
                for k in ORDER:
                    if r < splits(k):
                        back_side(h, k, r).wait_recv()
            at = inner(last, r)
            for k in range(Z):
                rows_s[h, pl.ds(k * group, group), at] = back_s[h, k, :, :, :, at].reshape(group, at.size)
            mix_out[h, r] = mixed(spreads[h], rows_s[h, :, at]).astype(BF16)
            finals[h, r] = remote(mix_out.at[h, r], mix_in.at[h, r], fin_s.at[h, r], fin_r.at[h, r], me, side[h])
            finals[h, r].start()
    for r in range(splits(last)):
        with jax.named_scope("bo"):
            for k in ORDER:
                if r < splits(k):
                    back_own(k, r).wait_recv()
        for h in range(2):
            at = cut(last, h, r)
            for k in range(Z):
                rows[pl.ds(k * group, group), at] = back_o[k, :, :, :, at].reshape(group, at.size)
            value = mixed(spread_own, rows[:, at])
            with jax.named_scope("fin"):
                finals[h, r].wait()
            out_ref[:, at] = (value + mix_in[h, r].astype(F32)).astype(BF16)

    for k in ORDER:
        for copy in posts(k):
            copy.wait_send()
        for r in range(splits(k)):
            for copy in returns(k, r):
                copy.wait_send()
            back_own(k, r).wait_send()
            for h in range(2):
                back_side(h, k, r).wait_send()
        for i, view in enumerate((fill_o.at[0], fill_s.at[0, 0], fill_s.at[1, 0])):
            drained(view, yz_s.at[i, k], yz_s.at[i, k], k).wait_send()


def per_device(tokens, norm_gain, expert_ids, route_weight, exp_gate, exp_up, exp_down):
    toks, width = tokens.shape
    half = width // 2
    inner = exp_gate.shape[2]
    ids = expert_ids.reshape(TP, toks, TOP).transpose(0, 2, 1)
    weight = route_weight.reshape(TP, toks, TOP).transpose(0, 2, 1)
    vmem, hbm = pl.BlockSpec(memory_space=pltpu.VMEM), pl.BlockSpec(memory_space=pl.ANY)
    dma = pltpu.SemaphoreType.DMA
    full, part = (YC, PAIRS, 2, width), (YC, PAIRS, 2, half)
    group = YC * CAP
    return pl.pallas_call(
        kernel,
        out_shape=jax.ShapeDtypeStruct((toks, width), BF16),
        in_specs=[vmem] * 4 + [hbm] * 3,
        out_specs=vmem,
        scratch_shapes=[
            pltpu.VMEM((width, inner), BF16),
            pltpu.VMEM((width, inner), BF16),
            pltpu.VMEM((inner, width), BF16),
            pltpu.VMEM((2, toks, half), BF16),
            pltpu.VMEM((2, toks, half), BF16),
            pltpu.VMEM((Z,) + full, BF16),
            pltpu.VMEM((2, Z) + part, BF16),
            pltpu.VMEM((TP, Z) + full, BF16),
            pltpu.VMEM((TP, Z) + full, BF16),
            pltpu.VMEM((TP * group, width), BF16),
            pltpu.VMEM((TP * group, inner), BF16),
            pltpu.VMEM((Z,) + full, BF16),
            pltpu.VMEM((2, Z) + part, BF16),
            pltpu.VMEM((Z,) + full, BF16),
            pltpu.VMEM((2, Z) + part, BF16),
            pltpu.VMEM((2, Z * group, half), BF16),
            pltpu.VMEM((2, 2, toks, half // 2), BF16),
            pltpu.VMEM((2, 2, toks, half // 2), BF16),
            dma((3,)),
            dma((2,)),
            dma((2,)),
            dma((3, Z)),
            dma((3, Z)),
            dma((4, Z)),
            dma((4, Z)),
            dma((4, Z + 1)),
            dma((4, Z + 1)),
            dma((3, Z + 1)),
            dma((3, Z + 1)),
            dma((2, 2)),
            dma((2, 2)),
        ],
        compiler_params=pltpu.CompilerParams(
            collective_id=0, has_side_effects=True, vmem_limit_bytes=63 * 2**20
        ),
    )(ids, weight, tokens, norm_gain.reshape(1, width), exp_gate, exp_up, exp_down)


def solution(mesh):
    return jax.shard_map(
        per_device,
        mesh=mesh,
        in_specs=(
            P(("ep", "tp"), None),
            P(),
            P("ep", None),
            P("ep", None),
            P("ep", None, "tp"),
            P("ep", None, "tp"),
            P("ep", "tp", None),
        ),
        out_specs=P(("ep", "tp"), None),
        check_vma=False,
    )
```

time: 129 us -> 105 us (0.81)
  Pallas kernels: 126 us -> 101 us
    pallas_call x1, Pallas kernels: 126 us -> 101 us  [per_device(): pl.pallas_call(kernel, out_shape=jax.ShapeDtypeStruct((toks, width), BF16...]
where the time goes in v2:
time: 105 us; the launch traced here: 103 us
  Pallas kernels  101 us (96%)
  local copies, waits for them, and re-layouts  1.88 us (2%)
    pallas_call x1, Pallas kernels, per_device(): pl.pallas_call(kernel, out_shape=jax.ShapeDtypeStruct((toks, width), BF16...  101 us

profile of v2, /device:TPU:0, one launch (start us, length us, event | category | flops | bytes accessed | tf_op | source)
XLA Modules:
  0.0 103.4 jit_solution(689188569814246999)
XLA Ops:
  0.0 101.5 %shard_map.73 = bf16[128,2048]{1,0:T(8,128)(2,1)} custom-call(s32[4,2,128]{2,1,0:T(2,128)} %bitcast.8, f32[4,2,128]{2,1,0:T(2,128)} %bitcast.9, bf16[128,2048]{1,0:T(8,128)(2,1)} %tok_ref.1, f32[1,2048]{1,0:T(1,128)} %bitcast.7, bf16[1,2048,1792]{2,1,0:T(8,128)(2,1)} %gate_hbm.1, bf16[1,2048,1792]{2,1,0:T(8,128)(2,1)} %up_hbm.1, bf16[1,1792,2048]{2,1,0:T(8,128)(2,1)} %down_hbm.1), custom_call_target="tpu_custom_call" | custom-call | tf_op jit(solution)/shard_map/pallas_call | solution.py:344
  101.5 1.9 %copy.9 = bf16[128,2048]{1,0:T(8,128)(2,1)} copy(bf16[128,2048]{1,0:T(8,128)(2,1)} %shard_map.73) | data formatting | bytes 1048576

commit v3 on v2

v3 whole, which is shorter than its diff:
```python
import jax
import jax.numpy as jnp
from jax import lax
from jax.experimental import pallas as pl
from jax.experimental.pallas import tpu as pltpu
from jax.sharding import PartitionSpec as P

TOP = 2
CAP = 10
EPS = 1e-05
Z, YC, TP = 4, 8, 4
PAIRS = CAP // 2
ORDER = (1, 0, 3, 2)
WIDE = 8
MESH = pl.DeviceIdType.MESH
BF16, F32 = jnp.bfloat16, jnp.float32


def kernel(
    ids_ref, weight_ref, gain_ref, tok_hbm, gate_hbm, up_hbm, down_hbm, out_ref,
    w_gate, w_up, w_down, tok, own_n, side_n, fill_o, fill_s, got, part, rows, hidden,
    ret_o, ret_s, back_o, back_s, rows_s, mix_out, mix_in, spreads,
    w_sem, pre_s, pre_r, yz_s, yz_r, xp_s, xp_r, xr_s, xr_r, yb_s, yb_r, fin_s, fin_r,
):
    me, x = lax.axis_index("ep"), lax.axis_index("tp")
    z, y, core = me // 8, me // 2 % 4, me % 2
    xr, xl, xo = (x + 1) % TP, (x + 3) % TP, (x + 2) % TP
    toks, full = own_n.shape
    wide = side_n.shape[2]
    half, rest, quarter = full // 2, full - wide, full // 4
    side = (xl, xr)
    group = YC * CAP
    tiles = hidden.shape[1] // 256

    barrier = pltpu.get_barrier_semaphore()

    @pl.loop(1, Z * YC)
    def _(i):
        pl.semaphore_signal(barrier, inc=1, device_id=((me + i) % (Z * YC), x), device_id_type=MESH)

    for peer in (xl, xr):
        pl.semaphore_signal(barrier, inc=1, device_id=(me, peer), device_id_type=MESH)

    sources = ((gate_hbm.at[0], w_gate), (up_hbm.at[0], w_up), (down_hbm.at[0], w_down), (tok_hbm, tok))
    loads = [pltpu.make_async_copy(src, dst, w_sem.at[i]) for i, (src, dst) in enumerate(sources)]
    loads[3].start()

    def remote(src, dst, send, recv, ep, tp):
        return pltpu.make_async_remote_copy(
            src_ref=src, dst_ref=dst, send_sem=send, recv_sem=recv, device_id=(ep, tp), device_id_type=MESH
        )

    def mirror(h, lo, hi):
        return (lo, hi) if h == 0 else (full - hi, full - lo)

    def cols(h, lo, hi, base=0):
        lo, hi = mirror(h, lo, hi)
        return pl.ds(lo - base, hi - lo)

    loads[3].wait()
    for load in loads[:3]:
        load.start()

    @pl.loop(0, toks // 32)
    def _(i):
        at = pl.ds(pl.multiple_of(i * 32, 32), 32)
        v = tok[at, :].astype(F32)
        factor = lax.rsqrt(jnp.mean(v * v, axis=-1, keepdims=True) + EPS)
        own_n[at, :] = (v * factor * gain_ref[...]).astype(BF16)

    with jax.named_scope("bar"):
        pl.semaphore_wait(barrier, Z * YC - 1 + 2)
    pres = [
        remote(own_n.at[:, cols(h, 0, wide)], side_n.at[h], pre_s.at[h], pre_r.at[h], me, (xr, xl)[h])
        for h in range(2)
    ]
    for copy in pres:
        copy.start()

    def targets(at):
        pair = ids_ref[at]
        e = lax.broadcasted_iota(jnp.int32, (Z * YC, toks), 0)
        before = lax.broadcasted_iota(jnp.int32, (toks, toks), 0) < lax.broadcasted_iota(jnp.int32, (toks, toks), 1)
        named = [e == pair[k : k + 1, :] for k in range(TOP)]
        member = (named[0] | named[1]).astype(F32).astype(BF16)
        count = jnp.dot(member, before.astype(F32).astype(BF16), preferred_element_type=F32)
        slots = [jnp.sum(jnp.where(n, count, 0.0), axis=0, keepdims=True).astype(jnp.int32) for n in named]
        dz = (z - (pair >> 3)) & 3
        k = (y - (pair >> 1) - dz) & 3
        base = ((k * 4 + dz) * 2 + (pair & 1)) * CAP
        return [base[k : k + 1, :] + slots[k] for k in range(TOP)]

    def pick(where, base):
        r = lax.broadcasted_iota(jnp.int32, (group, toks), 0) + base
        return ((r == where[0]) | (r == where[1])).astype(F32).astype(BF16)

    def filled(onehot, values):
        o = jnp.dot(onehot, values, preferred_element_type=F32).astype(BF16)
        return o.reshape(YC, PAIRS, 2, values.shape[1])

    def each(k, sign, send):
        @pl.loop(1 if k == 0 else 0, YC)
        def _(i):
            dz, c = i // 2, (core + i) % 2
            ep = (z + 4 + sign * dz) % 4 * 8 + (y + 8 + sign * (dz + k)) % 4 * 2 + c
            send(dz * 2 + c, dz * 2 + core, ep)

    def drained(view, send, recv, k):
        count = YC - 1 if k == 0 else YC
        return remote(view.at[pl.ds(0, count)], view.at[pl.ds(0, count)], send, recv, me, xr)

    where_own = targets(x)

    def fill_own(k):
        fill_o[k] = filled(pick(where_own, k * group), own_n[...])
        if k == 0:
            got[x, k, core] = fill_o[k, core]

    def send_own(k):
        def send(j, mine, ep):
            remote(fill_o.at[k, j], got.at[x, k, mine], yz_s.at[0, k], yz_r.at[0, k], ep, x).start()

        each(k, -1, send)

    def fill_side(k):
        for h in range(2):
            fill_s[h, k] = filled(pick(where_side[h], k * group), side_n[h])
            if k == 0:
                got[side[h], k, core, :, :, cols(h, 0, wide)] = fill_s[h, k, core]

    def send_side(k):
        def send(j, mine, ep):
            for h in range(2):
                remote(
                    fill_s.at[h, k, j], got.at[side[h], k, mine, :, :, cols(h, 0, wide)],
                    yz_s.at[1 + h, k], yz_r.at[1 + h, k], ep, x,
                ).start()

        each(k, -1, send)

    def post(k, i):
        t, h, to = ((x, 0, xl), (x, 1, xr), (xl, 0, xr), (xr, 1, xl))[i]
        at = cols(h, 0, half if i >= 2 else rest)
        ref = got.at[t, k, :, :, :, at]
        return remote(ref, ref, xp_s.at[i, k], xp_r.at[i, k], me, to)

    def forward_own(k):
        with jax.named_scope("fo"):
            drained(fill_o.at[0], yz_s.at[0, k], yz_r.at[0, k], k).wait_recv()
        for i in range(2):
            post(k, i).start()

    def forward_side(k):
        for h in range(2):
            with jax.named_scope("fs"):
                drained(fill_s.at[h, 0], yz_s.at[1 + h, k], yz_r.at[1 + h, k], k).wait_recv()
            post(k, 2 + h).start()

    k0, k1, k2, k3 = ORDER
    for k in ORDER:
        fill_own(k)
        send_own(k)
    where_side = [targets(side[h]) for h in range(2)]
    forward_own(k0)
    with jax.named_scope("pre"):
        for copy in pres:
            copy.wait()
    for k in ORDER:
        fill_side(k)
        send_side(k)
    forward_own(k1)

    for i, (at, where) in enumerate(((xl, where_side[0]), (xr, where_side[1]), (x, where_own))):
        r = lax.broadcasted_iota(jnp.int32, (Z * group, toks), 0)
        w = weight_ref[at]
        exact = jnp.where(r == where[0], w[0:1, :], 0.0) + jnp.where(r == where[1], w[1:2, :], 0.0)
        high = exact.astype(BF16)
        spreads[i, 0] = high
        spreads[i, 1] = (exact - high.astype(F32)).astype(BF16)

    forward_own(k2)
    forward_own(k3)

    def span(r):
        return ((0, quarter), (quarter, wide))[r]

    def own_spans(r):
        return [(0, quarter), (full - quarter, full)] if r == 0 else [(quarter, full - quarter)]

    def slot(k, r):
        return 2 * k + r

    def returns(k, r):
        i = slot(k, r)
        lo, hi = span(r)
        out = []
        for h in range(2):
            at = cols(h, lo, min(hi, rest))
            near, far = ((xr, xl), (xl, xr))[h]
            out.append(remote(part.at[near, k, :, :, :, at], ret_o.at[k, :, :, :, at], xr_s.at[2 * h, i], xr_r.at[2 * h, i], me, near))
            at, inner = cols(h, lo, min(hi, half)), cols(h, lo, min(hi, half), h * half)
            out.append(remote(part.at[xo, k, :, :, :, at], ret_s.at[h, k, :, :, :, inner], xr_s.at[2 * h + 1, i], xr_r.at[2 * h + 1, i], me, far))
        return out

    def up_phase(blocks, first, services):
        size = len(blocks) * group
        for i, (t, k) in enumerate(blocks):
            rows[pl.ds(i * group, group), :] = got[t, k].reshape(group, full)
        if first:
            loads[0].wait()
            loads[1].wait()
        for n in range(tiles):
            at = pl.ds(n * 256, 256)
            gate = jnp.dot(rows[:size, :], w_gate[:, at], preferred_element_type=F32)
            up = jnp.dot(rows[:size, :], w_up[:, at], preferred_element_type=F32)
            hidden[:size, at] = (gate / (1.0 + jnp.exp(-gate)) * up).astype(BF16)
            if n in services:
                services[n]()
        if first:
            loads[2].wait()

    def down_phase(blocks, lo, hi):
        size = len(blocks) * group
        at = pl.ds(lo, hi - lo)
        o = jnp.dot(hidden[:size, :], w_down[:, at], preferred_element_type=F32).astype(BF16)
        for i, (t, k) in enumerate(blocks):
            part[t, k, :, :, :, at] = o[i * group : (i + 1) * group].reshape(YC, PAIRS, 2, hi - lo)

    def give_back(k, r):
        lo, hi = span(r)
        with jax.named_scope("gw"):
            for copy in returns(k, r):
                copy.wait_recv()
        with jax.named_scope("gs"):

            @pl.loop(0, YC)
            def _(j):
                for h in range(2):
                    at = cols(h, lo, min(hi, rest))
                    part[x, k, j, :, :, at] = part[x, k, j, :, :, at] + ret_o[k, j, :, :, at]
                    at, inner = cols(h, lo, min(hi, half)), cols(h, lo, min(hi, half), h * half)
                    part[side[h], k, j, :, :, at] = part[side[h], k, j, :, :, at] + ret_s[h, k, j, :, :, inner]

        i = slot(k, r)
        views = [(part.at[side[h]], back_s.at[h], cols(h, lo, hi), cols(h, lo, hi, h * rest), 1 + h) for h in range(2)]
        views += [(part.at[x], back_o, pl.ds(a, b - a), pl.ds(a, b - a), 0) for a, b in own_spans(r)]
        if k == 0:
            for src, dst, at, inner, _ in views:
                dst[k, core, :, :, inner] = src[k, core, :, :, at]

        def send(j, mine, ep):
            for src, dst, at, inner, n in views:
                remote(src.at[k, j, :, :, at], dst.at[k, mine, :, :, inner], yb_s.at[n, i], yb_r.at[n, i], ep, x).start()

        each(k, 1, send)

    def chunk(k, services):
        blocks = [(t, k) for t in (xl, xr, xo)]
        with jax.named_scope("pw"):
            for i in range(4):
                post(k, i).wait_recv()
        with jax.named_scope("up"):
            up_phase(blocks, False, services)
        for r in range(2):
            with jax.named_scope("dn"):
                for lo, hi in own_spans(r):
                    down_phase(blocks, lo, hi)
            for copy in returns(k, r):
                copy.start()

    own = [(x, k) for k in ORDER]
    with jax.named_scope("upo"):
        up_phase(own, True, {3: lambda: forward_side(k0), 6: lambda: forward_side(k1)})
    with jax.named_scope("dno"):
        down_phase(own, 0, half)
        down_phase(own, half, full)
    chunk(k0, {2: lambda: forward_side(k2)})
    forward_side(k3)
    chunk(k1, {6: lambda: give_back(k0, 0)})
    chunk(k2, {0: lambda: give_back(k0, 1)})
    chunk(k3, {1: lambda: give_back(k1, 0), 6: lambda: give_back(k1, 1)})
    for k in (k2, k3):
        for r in range(2):
            give_back(k, r)

    def mixed(i, values):
        dims = (((0,), (0,)), ((), ()))
        return sum(lax.dot_general(spreads[i, n], values, dims, preferred_element_type=F32) for n in range(2))

    def back_side(h, k, r):
        lo, hi = span(r)
        view = fill_s.at[h, 0, :, :, :, pl.ds(0, hi - lo)]
        return drained(view, yb_s.at[1 + h, slot(k, r)], yb_r.at[1 + h, slot(k, r)], k)

    def back_own(k, r):
        view = fill_o.at[0, :, :, :, pl.ds(0, half)]
        return drained(view, yb_s.at[0, slot(k, r)], yb_r.at[0, slot(k, r)], k)

    finals = {}
    for r in range(2):
        lo, hi = span(r)
        for h in range(2):
            with jax.named_scope("bs"):
                for k in ORDER:
                    back_side(h, k, r).wait_recv()
            at = cols(h, lo, hi, h * rest)
            for k in range(Z):
                rows_s[h, pl.ds(k * group, group), at] = back_s[h, k, :, :, :, at].reshape(group, hi - lo)
            mix_out[h, :, at] = mixed(h, rows_s[h, :, at]).astype(BF16)
            finals[h, r] = remote(mix_out.at[h, :, at], mix_in.at[h, :, at], fin_s.at[h, r], fin_r.at[h, r], me, side[h])
            finals[h, r].start()
    for r in range(2):
        with jax.named_scope("bo"):
            for k in ORDER:
                back_own(k, r).wait_recv()
        for lo, hi in own_spans(r):
            at = pl.ds(lo, hi - lo)
            for k in range(Z):
                rows[pl.ds(k * group, group), at] = back_o[k, :, :, :, at].reshape(group, hi - lo)
        with jax.named_scope("fin"):
            for h in range(2):
                finals[h, r].wait()
        edges = sorted({e for lo, hi in own_spans(r) for e in (lo, hi)} | ({rest, wide} if r == 1 else set()))
        for lo, hi in zip(edges, edges[1:]):
            if r == 0 and lo == quarter:
                continue
            value = mixed(2, rows[:, lo:hi])
            if hi <= wide:
                value = value + mix_in[0, :, lo:hi].astype(F32)
            if lo >= rest:
                value = value + mix_in[1, :, lo - rest : hi - rest].astype(F32)
            out_ref[:, lo:hi] = value.astype(BF16)

    for k in ORDER:
        for i in range(4):
            post(k, i).wait_send()
        for r in range(2):
            for copy in returns(k, r):
                copy.wait_send()
            back_own(k, r).wait_send()
            for h in range(2):
                back_side(h, k, r).wait_send()
        for i, view in enumerate((fill_o.at[0], fill_s.at[0, 0], fill_s.at[1, 0])):
            drained(view, yz_s.at[i, k], yz_s.at[i, k], k).wait_send()


def per_device(tokens, norm_gain, expert_ids, route_weight, exp_gate, exp_up, exp_down):
    toks, width = tokens.shape
    half = width // 2
    wide = WIDE * width // 16
    inner = exp_gate.shape[2]
    ids = expert_ids.reshape(TP, toks, TOP).transpose(0, 2, 1)
    weight = route_weight.reshape(TP, toks, TOP).transpose(0, 2, 1)
    vmem, hbm = pl.BlockSpec(memory_space=pltpu.VMEM), pl.BlockSpec(memory_space=pl.ANY)
    dma = pltpu.SemaphoreType.DMA
    group = YC * CAP

    def copies(*lead, size=width):
        return pltpu.VMEM(lead + (YC, PAIRS, 2, size), BF16)

    return pl.pallas_call(
        kernel,
        out_shape=pltpu.VMEM((toks, width), BF16),
        in_specs=[vmem] * 3 + [hbm] * 4,
        out_specs=vmem,
        scratch_shapes=[
            pltpu.VMEM((width, inner), BF16),
            pltpu.VMEM((width, inner), BF16),
            pltpu.VMEM((inner, width), BF16),
            pltpu.VMEM((toks, width), BF16),
            pltpu.VMEM((toks, width), BF16),
            pltpu.VMEM((2, toks, wide), BF16),
            copies(Z),
            copies(2, Z, size=wide),
            copies(TP, Z),
            copies(TP, Z),
            pltpu.VMEM((TP * group, width), BF16),
            pltpu.VMEM((TP * group, inner), BF16),
            copies(Z),
            copies(2, Z, size=half),
            copies(Z),
            copies(2, Z, size=wide),
            pltpu.VMEM((2, Z * group, wide), BF16),
            pltpu.VMEM((2, toks, wide), BF16),
            pltpu.VMEM((2, toks, wide), BF16),
            pltpu.VMEM((3, 2, Z * group, toks), BF16),
            dma((4,)),
            dma((2,)),
            dma((2,)),
            dma((3, Z)),
            dma((3, Z)),
            dma((4, Z)),
            dma((4, Z)),
            dma((4, 2 * Z)),
            dma((4, 2 * Z)),
            dma((3, 2 * Z)),
            dma((3, 2 * Z)),
            dma((2, 2)),
            dma((2, 2)),
        ],
        compiler_params=pltpu.CompilerParams(
            collective_id=0, has_side_effects=True, vmem_limit_bytes=63 * 2**20
        ),
    )(ids, weight, norm_gain.reshape(1, width), tokens, exp_gate, exp_up, exp_down)


def solution(mesh):
    return jax.shard_map(
        per_device,
        mesh=mesh,
        in_specs=(
            P(("ep", "tp"), None),
            P(),
            P("ep", None),
            P("ep", None),
            P("ep", None, "tp"),
            P("ep", None, "tp"),
            P("ep", "tp", None),
        ),
        out_specs=P(("ep", "tp"), None),
        check_vma=False,
    )
```

time: 105 us -> 97.1 us (0.925)
  Pallas kernels: 101 us -> 94.5 us
  local copies, waits for them, and re-layouts: 1.88 us -> 0.8 us
    pallas_call x1, Pallas kernels: 101 us -> 94.5 us  [per_device(): pl.pallas_call(kernel, out_shape=pltpu.VMEM((toks, width), BF16), in_spec...]
    unnamed x1, local copies, waits for them, and re-layouts: 1.88 us -> 0.8 us
where the time goes in v3:
time: 97.1 us; the launch traced here: 95.3 us
  Pallas kernels  94.5 us (97%)
    pallas_call x1, Pallas kernels, per_device(): pl.pallas_call(kernel, out_shape=pltpu.VMEM((toks, width), BF16), in_spec...  94.5 us

profile of v3, /device:TPU:0, one launch (start us, length us, event | category | flops | bytes accessed | tf_op | source)
XLA Modules:
  0.0 95.3 jit_solution(5155907113857088622)
XLA Ops:
  0.0 94.5 %shard_map.73 = bf16[128,2048]{1,0:T(8,128)(2,1)S(1)} custom-call(s32[4,2,128]{2,1,0:T(2,128)} %bitcast.8, f32[4,2,128]{2,1,0:T(2,128)} %bitcast.9, f32[1,2048]{1,0:T(1,128)} %bitcast.7, bf16[128,2048]{1,0:T(8,128)(2,1)} %tok_hbm.1, bf16[1,2048,1792]{2,1,0:T(8,128)(2,1)} %gate_hbm.1, bf16[1,2048,1792]{2,1,0:T(8,128)(2,1)} %up_hbm.1, ...), custom_call_target="tpu_custom_call" | custom-call | tf_op jit(solution)/shard_map/pallas_call | solution.py:361
  94.5 0.8 copy.9

commit v4 on v3

--- a/solution.py
+++ b/solution.py
@@ -12,6 +12,7 @@
 PAIRS = CAP // 2
 ORDER = (1, 0, 3, 2)
 WIDE = 8
+CUTS = (0, 4)
 MESH = pl.DeviceIdType.MESH
 BF16, F32 = jnp.bfloat16, jnp.float32
 
@@ -19,7 +20,7 @@
 def kernel(
     ids_ref, weight_ref, gain_ref, tok_hbm, gate_hbm, up_hbm, down_hbm, out_ref,
     w_gate, w_up, w_down, tok, own_n, side_n, fill_o, fill_s, got, part, rows, hidden,
-    ret_o, ret_s, back_o, back_s, rows_s, mix_out, mix_in, spreads,
+    ret_o, ret_s, back_o, back_s, rows_s, mix_out, mix_in, spreads, own_mix,
     w_sem, pre_s, pre_r, yz_s, yz_r, xp_s, xp_r, xr_s, xr_r, yb_s, yb_r, fin_s, fin_r,
 ):
     me, x = lax.axis_index("ep"), lax.axis_index("tp")
@@ -27,7 +28,7 @@
     xr, xl, xo = (x + 1) % TP, (x + 3) % TP, (x + 2) % TP
     toks, full = own_n.shape
     wide = side_n.shape[2]
-    half, rest, quarter = full // 2, full - wide, full // 4
+    half, rest = full // 2, full - wide
     side = (xl, xr)
     group = YC * CAP
     tiles = hidden.shape[1] // 256
@@ -181,14 +182,18 @@
     forward_own(k2)
     forward_own(k3)
 
+    bounds = [c * full // 16 for c in CUTS] + [wide]
+    turns = len(CUTS)
+
     def span(r):
-        return ((0, quarter), (quarter, wide))[r]
+        return bounds[r], bounds[r + 1]
 
     def own_spans(r):
-        return [(0, quarter), (full - quarter, full)] if r == 0 else [(quarter, full - quarter)]
+        lo, hi = span(r)
+        return [(lo, full - lo)] if r == turns - 1 else [(lo, hi), (full - hi, full - lo)]
 
     def slot(k, r):
-        return 2 * k + r
+        return turns * k + r
 
     def returns(k, r):
         i = slot(k, r)
@@ -226,24 +231,8 @@
         for i, (t, k) in enumerate(blocks):
             part[t, k, :, :, :, at] = o[i * group : (i + 1) * group].reshape(YC, PAIRS, 2, hi - lo)
 
-    def give_back(k, r):
-        lo, hi = span(r)
-        with jax.named_scope("gw"):
-            for copy in returns(k, r):
-                copy.wait_recv()
-        with jax.named_scope("gs"):
-
-            @pl.loop(0, YC)
-            def _(j):
-                for h in range(2):
-                    at = cols(h, lo, min(hi, rest))
-                    part[x, k, j, :, :, at] = part[x, k, j, :, :, at] + ret_o[k, j, :, :, at]
-                    at, inner = cols(h, lo, min(hi, half)), cols(h, lo, min(hi, half), h * half)
-                    part[side[h], k, j, :, :, at] = part[side[h], k, j, :, :, at] + ret_s[h, k, j, :, :, inner]
-
+    def send_views(k, r, views):
         i = slot(k, r)
-        views = [(part.at[side[h]], back_s.at[h], cols(h, lo, hi), cols(h, lo, hi, h * rest), 1 + h) for h in range(2)]
-        views += [(part.at[x], back_o, pl.ds(a, b - a), pl.ds(a, b - a), 0) for a, b in own_spans(r)]
         if k == 0:
             for src, dst, at, inner, _ in views:
                 dst[k, core, :, :, inner] = src[k, core, :, :, at]
@@ -253,6 +242,41 @@
                 remote(src.at[k, j, :, :, at], dst.at[k, mine, :, :, inner], yb_s.at[n, i], yb_r.at[n, i], ep, x).start()
 
         each(k, 1, send)
+
+    def side_sum(k, r, j):
+        lo, hi = span(r)
+        for h in range(2):
+            at, inner = cols(h, lo, min(hi, half)), cols(h, lo, min(hi, half), h * half)
+            part[side[h], k, j, :, :, at] = part[side[h], k, j, :, :, at] + ret_s[h, k, j, :, :, inner]
+
+    def own_sum(k, r, j):
+        lo, hi = span(r)
+        for h in range(2):
+            at = cols(h, lo, min(hi, rest))
+            part[x, k, j, :, :, at] = part[x, k, j, :, :, at] + ret_o[k, j, :, :, at]
+
+    def side_views(r):
+        lo, hi = span(r)
+        return [(part.at[side[h]], back_s.at[h], cols(h, lo, hi), cols(h, lo, hi, h * rest), 1 + h) for h in range(2)]
+
+    def own_views(r):
+        return [(part.at[x], back_o, pl.ds(a, b - a), pl.ds(a, b - a), 0) for a, b in own_spans(r)]
+
+    def give_back(k, r, which=("side", "own")):
+        with jax.named_scope("gw"):
+            copies = returns(k, r)
+            for copy in (copies[1::2] if "side" in which else []) + (copies[::2] if "own" in which else []):
+                copy.wait_recv()
+        with jax.named_scope("gs"):
+
+            @pl.loop(0, YC)
+            def _(j):
+                if "side" in which:
+                    side_sum(k, r, j)
+                if "own" in which:
+                    own_sum(k, r, j)
+
+        send_views(k, r, (side_views(r) if "side" in which else []) + (own_views(r) if "own" in which else []))
 
     def chunk(k, services):
         blocks = [(t, k) for t in (xl, xr, xo)]
@@ -261,12 +285,17 @@
                 post(k, i).wait_recv()
         with jax.named_scope("up"):
             up_phase(blocks, False, services)
-        for r in range(2):
+        for r in range(turns):
             with jax.named_scope("dn"):
                 for lo, hi in own_spans(r):
                     down_phase(blocks, lo, hi)
-            for copy in returns(k, r):
+            copies = returns(k, r)
+            for copy in copies[1::2] + (copies[::2] if k != k3 else []):
                 copy.start()
+        if k == k3:
+            for r in range(turns):
+                for copy in returns(k, r)[::2]:
+                    copy.start()
 
     own = [(x, k) for k in ORDER]
     with jax.named_scope("upo"):
@@ -276,12 +305,19 @@
         down_phase(own, half, full)
     chunk(k0, {2: lambda: forward_side(k2)})
     forward_side(k3)
-    chunk(k1, {6: lambda: give_back(k0, 0)})
-    chunk(k2, {0: lambda: give_back(k0, 1)})
-    chunk(k3, {1: lambda: give_back(k1, 0), 6: lambda: give_back(k1, 1)})
-    for k in (k2, k3):
-        for r in range(2):
+    def give(k, *which):
+        for r in which:
             give_back(k, r)
+
+    later = range(1, turns)
+    chunk(k1, {6: lambda: give(k0, 0)})
+    chunk(k2, {0: lambda: give(k0, *later)})
+    chunk(k3, {1: lambda: give(k1, 0), 6: lambda: give(k1, *later)})
+    give(k2, *range(turns - 1))
+    tail = ((k2, turns - 1), *((k3, r) for r in range(turns)))
+    for which in ("side", "own"):
+        for k, r in tail:
+            give_back(k, r, (which,))
 
     def mixed(i, values):
         dims = (((0,), (0,)), ((), ()))
@@ -293,11 +329,11 @@
         return drained(view, yb_s.at[1 + h, slot(k, r)], yb_r.at[1 + h, slot(k, r)], k)
 
     def back_own(k, r):
-        view = fill_o.at[0, :, :, :, pl.ds(0, half)]
+        view = fill_o.at[0, :, :, :, pl.ds(0, sum(hi - lo for lo, hi in own_spans(r)))]
         return drained(view, yb_s.at[0, slot(k, r)], yb_r.at[0, slot(k, r)], k)
 
     finals = {}
-    for r in range(2):
+    for r in range(turns):
         lo, hi = span(r)
         for h in range(2):
             with jax.named_scope("bs"):
@@ -309,7 +345,7 @@
             mix_out[h, :, at] = mixed(h, rows_s[h, :, at]).astype(BF16)
             finals[h, r] = remote(mix_out.at[h, :, at], mix_in.at[h, :, at], fin_s.at[h, r], fin_r.at[h, r], me, side[h])
             finals[h, r].start()
-    for r in range(2):
+    for r in range(turns):
         with jax.named_scope("bo"):
             for k in ORDER:
                 back_own(k, r).wait_recv()
@@ -317,14 +353,17 @@
             at = pl.ds(lo, hi - lo)
             for k in range(Z):
                 rows[pl.ds(k * group, group), at] = back_o[k, :, :, :, at].reshape(group, hi - lo)
+            own_mix[:, at] = mixed(2, rows[:, at])
+    for r in range(turns):
         with jax.named_scope("fin"):
             for h in range(2):
                 finals[h, r].wait()
-        edges = sorted({e for lo, hi in own_spans(r) for e in (lo, hi)} | ({rest, wide} if r == 1 else set()))
-        for lo, hi in zip(edges, edges[1:]):
-            if r == 0 and lo == quarter:
-                continue
-            value = mixed(2, rows[:, lo:hi])
+        spans = own_spans(r)
+        if r == turns - 1:
+            edges = sorted({rest, wide, *spans[0]})
+            spans = list(zip(edges, edges[1:]))
+        for lo, hi in spans:
+            value = own_mix[:, lo:hi]
             if hi <= wide:
                 value = value + mix_in[0, :, lo:hi].astype(F32)
             if lo >= rest:
@@ -334,7 +373,7 @@
     for k in ORDER:
         for i in range(4):
             post(k, i).wait_send()
-        for r in range(2):
+        for r in range(turns):
             for copy in returns(k, r):
                 copy.wait_send()
             back_own(k, r).wait_send()
@@ -384,6 +423,7 @@
             pltpu.VMEM((2, toks, wide), BF16),
             pltpu.VMEM((2, toks, wide), BF16),
             pltpu.VMEM((3, 2, Z * group, toks), BF16),
+            pltpu.VMEM((toks, width), F32),
             dma((4,)),
             dma((2,)),
             dma((2,)),
@@ -391,12 +431,12 @@
             dma((3, Z)),
             dma((4, Z)),
             dma((4, Z)),
-            dma((4, 2 * Z)),
-            dma((4, 2 * Z)),
-            dma((3, 2 * Z)),
-            dma((3, 2 * Z)),
-            dma((2, 2)),
-            dma((2, 2)),
+            dma((4, len(CUTS) * Z)),
+            dma((4, len(CUTS) * Z)),
+            dma((3, len(CUTS) * Z)),
+            dma((3, len(CUTS) * Z)),
+            dma((2, len(CUTS))),
+            dma((2, len(CUTS))),
         ],
         compiler_params=pltpu.CompilerParams(
             collective_id=0, has_side_effects=True, vmem_limit_bytes=63 * 2**20

time: 97.1 us -> 94.6 us (0.974)
  the two profiles are of different devices: /device:TPU:0 before, /device:TPU:114 now
where the time goes in v4:
time: 94.6 us; the launch traced here: 94.4 us
  Pallas kernels  93.6 us (99%)
    pallas_call x1, Pallas kernels, per_device(): pl.pallas_call(kernel, out_shape=pltpu.VMEM((toks, width), BF16), in_spec...  93.6 us

profile of v4, /device:TPU:114, one launch (start us, length us, event | category | flops | bytes accessed | tf_op | source)
XLA Modules:
  0.0 94.4 jit_solution(17077782903513564597)
XLA Ops:
  0.0 93.6 %shard_map.73 = bf16[128,2048]{1,0:T(8,128)(2,1)S(1)} custom-call(s32[4,2,128]{2,1,0:T(2,128)} %bitcast.8, f32[4,2,128]{2,1,0:T(2,128)} %bitcast.9, f32[1,2048]{1,0:T(1,128)} %bitcast.7, bf16[128,2048]{1,0:T(8,128)(2,1)} %tok_hbm.1, bf16[1,2048,1792]{2,1,0:T(8,128)(2,1)} %gate_hbm.1, bf16[1,2048,1792]{2,1,0:T(8,128)(2,1)} %up_hbm.1, ...), custom_call_target="tpu_custom_call" | custom-call | tf_op jit(solution)/shard_map/pallas_call | solution.py:400
  93.6 0.8 copy.9
